TPU v7x, 32 devices: a whole 2x2x4 slice. The times are simulated.
32 devices in a mesh: kv: 8 (over z, y), tp: 4 (over x, core).
Axes of the slice: x: 2, y: 2, z: 4, core: 2. Of those that a mesh axis runs over, the one named last changes fastest.
Arguments:
- piece_tokens: bfloat16 [32, 2048], P('kv'), may hold values from -6 to 6
- decode_tokens: bfloat16 [8, 2048], P('kv'), may hold values from -6 to 6
- prompt_fill: int32 [1], replicated, may hold values from 1024 to 2016
- decode_fill: int32 [8], P('kv'), may hold values from 1 to 767, 3072 in all
- prompt_cache: bfloat16 [2048, 544], P('kv'), may hold values from -600 to 600
- decode_cache: bfloat16 [8, 768, 544], P('kv'), may hold values from -600 to 600
- input_gain: float32 [2048], replicated, may hold values from 0.1 to 1.9
- query_gain: float32 [768], replicated, may hold values from 0.1 to 1.9
- latent_gain: float32 [512], replicated, may hold values from 0.1 to 1.9
- query_down: bfloat16 [2048, 768], P(None, 'tp'), may hold values from -0.125 to 0.125
- latent_down: bfloat16 [2048, 512], P(None, 'tp'), may hold values from -0.125 to 0.125
- rope_down: bfloat16 [2048, 32], replicated, may hold values from -0.125 to 0.125
- query_up: bfloat16 [768, 1024], P(None, 'tp'), may hold values from -0.21875 to 0.21875
- qrope_up: bfloat16 [768, 512], P(None, 'tp'), may hold values from -0.21875 to 0.21875
- key_up: bfloat16 [16, 64, 512], P('tp'), may hold values from -0.25 to 0.25
- value_up: bfloat16 [16, 512, 64], P('tp'), may hold values from -4 to 4
- out_proj: bfloat16 [1024, 2048], P('tp'), may hold values from -4 to 4
Outputs:
- piece_out: bfloat16 [32, 2048], P('kv')
- decode_out: bfloat16 [8, 2048], P('kv')
- piece_rows: bfloat16 [32, 544], P('kv')
- decode_rows: bfloat16 [8, 544], P('kv')
Inputs may be any that keep to these rules, and one draw needn't show every extreme that they name: `prompt_fill`: the piece takes the 32 positions that follow the cache's filled positions. `decode_fill`: a decoding sequence's new token takes the position that follows its filled ones.
All inputs are finite; a program needn't handle non-finite values. No bound on the sum of `decode_fill` on one device may be relied on, other than what follows from the above.
Results may differ from a plain program's by a relative error of at most 0.035.
Values may be sent and summed in bfloat16 or wider, within the bound.
A program may use at most 64 MiB of HBM per device.

v0:
```python
import jax
import jax.numpy as jnp
from jax import lax
from jax.sharding import PartitionSpec as P

NOPE = 64
ROPE = 32
NEG_FILL = -1e30
RMS_EPS = 1e-06
THETA = 10000.0


def rms_scale(values, gain_row):
    widened = values.astype(jnp.float32)
    scaled = (
        widened
        * lax.rsqrt(jnp.mean(widened * widened, axis=-1, keepdims=True) + RMS_EPS)
        * gain_row
    )
    return scaled.astype(jnp.bfloat16)


def rotate(values, places):
    half_width = values.shape[-1] // 2
    inverse = THETA ** (-jnp.arange(half_width, dtype=jnp.float32) / half_width)
    angles = places.astype(jnp.float32)[..., None] * inverse
    first_half = values[..., :half_width].astype(jnp.float32)
    second_half = values[..., half_width:].astype(jnp.float32)
    cosine = jnp.cos(angles)
    sine_part = jnp.sin(angles)
    return jnp.concatenate(
        [
            first_half * cosine - second_half * sine_part,
            first_half * sine_part + second_half * cosine,
        ],
        axis=-1,
    ).astype(jnp.bfloat16)


def make_queries(query_lat, places, query_up, qrope_up, key_up):
    row_count = query_lat.shape[0]
    head_count = key_up.shape[0]
    nope_part = (
        jnp.dot(query_lat, query_up, preferred_element_type=jnp.float32)
        .astype(jnp.bfloat16)
        .reshape(row_count, head_count, -1)
    )
    rope_raw = (
        jnp.dot(query_lat, qrope_up, preferred_element_type=jnp.float32)
        .astype(jnp.bfloat16)
        .reshape(row_count, head_count, -1)
    )
    turned = rotate(rope_raw, places[:, None])
    absorbed = jnp.einsum(
        "nhc,hcl->nhl", nope_part, key_up, preferred_element_type=jnp.float32
    ).astype(jnp.bfloat16)
    return (absorbed, turned)


def block_attend(absorbed, turned, key_rows, key_places, query_places, value_up):
    latent_width = value_up.shape[1]
    score_scale = (NOPE + ROPE) ** (-0.5)
    latent_keys = key_rows[:, :latent_width]
    scores = (
        jnp.einsum("nhl,sl->nhs", absorbed, latent_keys, preferred_element_type=jnp.float32)
        + jnp.einsum(
            "nhr,sr->nhs", turned, key_rows[:, latent_width:], preferred_element_type=jnp.float32
        )
    ) * score_scale
    allowed = key_places[None, None, :] <= query_places[:, None, None]
    scores = jnp.where(allowed, scores, NEG_FILL)
    local_peak = jnp.max(scores, axis=-1)
    exp_scores = jnp.where(allowed, jnp.exp(scores - local_peak[..., None]), 0.0)
    weight_sum = jnp.sum(exp_scores, axis=-1)
    weights = exp_scores.astype(jnp.bfloat16)
    mixed_rows = jnp.einsum("nhs,sl->nhl", weights, latent_keys, preferred_element_type=jnp.float32)
    partial_sum = jnp.einsum(
        "nhl,hlv->nhv", mixed_rows, value_up.astype(jnp.float32), precision=lax.Precision.HIGHEST
    )
    return (partial_sum, weight_sum, local_peak)


def insert_row(cache_rows, new_row, fill_one):
    return lax.dynamic_update_slice(cache_rows, new_row[None], (fill_one, jnp.zeros((), jnp.int32)))


def local(
    piece_tokens,
    decode_tokens,
    prompt_fill,
    decode_fill,
    prompt_cache,
    decode_cache,
    input_gain,
    query_gain,
    latent_gain,
    query_down,
    latent_down,
    rope_down,
    query_up,
    qrope_up,
    key_up,
    value_up,
    out_proj,
):
    kv_index = lax.axis_index("kv")
    piece_dev = piece_tokens.shape[0]
    shard_len = prompt_cache.shape[0]
    fill_start = prompt_fill[0]
    own_places = fill_start + kv_index * piece_dev + jnp.arange(piece_dev, dtype=jnp.int32)
    places = jnp.concatenate([own_places, decode_fill])
    tokens = jnp.concatenate([piece_tokens, decode_tokens], axis=0)
    normed = rms_scale(tokens, input_gain)
    query_comp = jnp.dot(normed, query_down, preferred_element_type=jnp.float32).astype(
        jnp.bfloat16
    )
    latent_comp = jnp.dot(normed, latent_down, preferred_element_type=jnp.float32).astype(
        jnp.bfloat16
    )
    query_comp, latent_comp = (
        lax.all_gather(query_comp, "tp", axis=1, tiled=True),
        lax.all_gather(latent_comp, "tp", axis=1, tiled=True),
    )
    query_lat = rms_scale(query_comp, query_gain)
    rope_raw = jnp.dot(normed, rope_down, preferred_element_type=jnp.float32).astype(jnp.bfloat16)
    new_rows = jnp.concatenate(
        [rms_scale(latent_comp, latent_gain), rotate(rope_raw, places)], axis=-1
    )
    piece_rows = new_rows[:piece_dev]
    decode_rows = new_rows[piece_dev:]
    decode_absorbed, decode_turned = make_queries(
        query_lat[piece_dev:], decode_fill, query_up, qrope_up, key_up
    )
    piece_latent, arrived = (
        lax.all_gather(query_lat[:piece_dev], "kv", axis=0, tiled=True),
        lax.all_gather(piece_rows, "kv", axis=0, tiled=True),
    )
    arrived_places = fill_start + jnp.arange(arrived.shape[0], dtype=jnp.int32)
    piece_absorbed, piece_turned = make_queries(
        piece_latent, arrived_places, query_up, qrope_up, key_up
    )
    piece_total = arrived.shape[0]
    query_places = fill_start + jnp.arange(piece_total, dtype=jnp.int32)
    zero_rows = jnp.zeros((shard_len, arrived.shape[1]), arrived.dtype)
    padded = jnp.concatenate([zero_rows, arrived, zero_rows], axis=0)
    offset = jnp.clip(kv_index * shard_len - fill_start + shard_len, 0, piece_total + shard_len)
    window = lax.dynamic_slice_in_dim(padded, offset, shard_len, 0)
    key_places = kv_index * shard_len + jnp.arange(shard_len, dtype=jnp.int32)
    fresh_rows = (key_places >= fill_start) & (key_places < fill_start + piece_total)
    key_rows = jnp.where(fresh_rows[:, None], window, prompt_cache)
    partial_sum, weight_sum, local_peak = block_attend(
        piece_absorbed, piece_turned, key_rows, key_places, query_places, value_up
    )
    all_parts, all_totals, all_peaks = (
        lax.all_to_all(
            partial_sum.reshape(1, piece_total, -1), "kv", split_axis=1, concat_axis=0, tiled=True
        ),
        lax.all_to_all(weight_sum[None], "kv", split_axis=1, concat_axis=0, tiled=True),
        lax.all_to_all(local_peak[None], "kv", split_axis=1, concat_axis=0, tiled=True),
    )
    global_peak = jnp.max(all_peaks, axis=0)
    factor = jnp.exp(all_peaks - global_peak[None])
    merged = jnp.sum(all_parts.reshape(all_peaks.shape + (-1,)) * factor[..., None], axis=0)
    denominator = jnp.sum(all_totals * factor, axis=0)
    piece_value = (merged / denominator[..., None]).astype(jnp.bfloat16)
    decode_keys = jax.vmap(insert_row)(decode_cache, decode_rows, decode_fill)

    def attend_one(absorbed_one, turned_one, keys_one, fill_one):
        cache_places = jnp.arange(keys_one.shape[0], dtype=jnp.int32)
        return block_attend(
            absorbed_one[None], turned_one[None], keys_one, cache_places, fill_one[None], value_up
        )

    decode_part, decode_total, decode_peak = jax.vmap(attend_one)(
        decode_absorbed, decode_turned, decode_keys, decode_fill
    )
    decode_value = (decode_part[:, 0] / decode_total[:, 0, :, None]).astype(jnp.bfloat16)
    values = jnp.concatenate([piece_value, decode_value], axis=0)
    values = values.reshape(values.shape[0], -1)
    partial_value = jnp.dot(values, out_proj, preferred_element_type=jnp.float32).astype(
        jnp.bfloat16
    )
    summed = lax.psum(partial_value, "tp").astype(jnp.float32).astype(jnp.bfloat16)
    return (summed[:piece_dev], summed[piece_dev:], piece_rows, decode_rows)


def solution(mesh):
    placed = (
        P("kv", None),
        P("kv", None),
        P(),
        P("kv"),
        P("kv", None),
        P("kv", None, None),
        P(),
        P(),
        P(),
        P(None, "tp"),
        P(None, "tp"),
        P(),
        P(None, "tp"),
        P(None, "tp"),
        P("tp", None, None),
        P("tp", None, None),
        P("tp", None),
    )
    return jax.shard_map(
        local,
        mesh=mesh,
        in_specs=placed,
        out_specs=(P("kv", None), P("kv", None), P("kv", None), P("kv", None)),
        check_vma=False,
    )
```

profile of v0, /device:TPU:0, one launch (start us, length us, event | category | flops | bytes accessed | tf_op | source)
XLA Modules:
  0.0 135.7 jit_solution(8345209168863359578)
XLA Ops:
  0.7 1.3 copy.80
  3.6 0.2 convolution_convert_fusion.6
  3.8 0.2 convolution_convert_fusion.5
  4.0 6.2 %all_gather.14 = bf16[5,512]{1,0:T(8,128)(2,1)S(1)} all-gather(bf16[5,128]{1,0:T(8,128)(2,1)S(1)} %convolution_convert_fusion.5), channel_id=1, replica_groups=mesh['kv'=8,'tp'=4] {'tp'}, dimensions={1}, use_global_device_ids=true | all-gather | bytes 6400 | tf_op jit(solution)/shard_map/all_gather | solution.py:122
  10.3 0.3 fusion.5
  10.6 5.5 %all-gather = bf16[4,192,5]{1,2,0:T(8,128)(2,1)S(1)} all-gather(bf16[1,192,5]{1,2,0:T(8,128)(2,1)S(1)} %fusion.5), channel_id=1, replica_groups=mesh['kv'=8,'tp'=4] {'tp'}, dimensions={0}, use_global_device_ids=true | all-gather | bytes 9600 | tf_op jit(solution)/shard_map/all_gather | solution.py:121
  16.4 0.2 copy.37
  16.7 0.6 copy-done.12
  17.6 31.4 %all-gather.2 = bf16[8,4,544]{2,1,0:T(4,128)(2,1)S(1)} all-gather(bf16[1,4,544]{2,1,0:T(4,128)(2,1)S(1)} %slice_bitcast_fusion.14), channel_id=1, replica_groups=mesh['kv'=8,'tp'=4] {'kv'}, dimensions={0}, use_global_device_ids=true | all-gather | bytes 39168 | tf_op jit(solution)/shard_map/all_gather | solution.py:136
  49.2 30.8 %all-gather.1 = bf16[8,4,768]{2,1,0:T(4,128)(2,1)S(1)} all-gather(bf16[1,4,768]{2,1,0:T(4,128)(2,1)S(1)} %slice_bitcast_fusion.10), channel_id=1, replica_groups=mesh['kv'=8,'tp'=4] {'kv'}, dimensions={0}, use_global_device_ids=true | all-gather | bytes 55296 | tf_op jit(solution)/shard_map/all_gather | solution.py:135
  80.0 0.1 convolution_convert_fusion.3
  80.4 0.2 convolution_convert_fusion.2
  80.9 0.9 fusion.10
  81.7 0.2 fusion.22
  81.9 0.7 copy-done.2
  82.7 0.4 fusion.76
  83.0 0.2 fusion.12
  83.2 0.7 copy.46
  83.9 5.4 %all-to-all-start.2 = ((f32[1,32,4]{2,0,1:T(1,128)}), f32[1,32,4]{2,0,1:T(1,128)S(1)}, u32[]{:S(2)}, u32[]{:S(2)}) async-start(f32[1,32,4]{2,0,1:T(1,128)} %copy.46), calls=%async_computation.2 | async-start | bytes 32768 | tf_op jit(solution)/shard_map/all_to_all | solution.py:158
  89.5 0.2 fusion.6
  89.7 0.2 fusion.11
  89.9 0.6 copy-done.14
  90.7 0.6 fusion.74
  91.3 0.8 constant_dynamic-slice_fusion
  92.1 0.7 copy-done.13
  92.8 2.0 %and_reduce_fusion = pred[]{:T(512)} fusion(s32[3]{0:T(128)S(1)} %copy-done.13, s32[1]{0:T(128)} %bitcast.20, s32[1]{0:T(128)} %bitcast.19, s32[1]{0:T(128)} %constant.79.clone.1), kind=kLoop, calls=%fused_computation.108 | loop fusion | flops 17 | bytes 25 | tf_op jit(solution)/shard_map/reduce.1
  94.8 1.2 broadcast_select_fusion
  96.0 0.2 copy.50
  96.2 1.6 %scatter.4 = bf16[1,768,544]{1,2,0:T(8,128)(2,1)S(1)} dynamic-update-slice(bf16[1,768,544]{1,2,0:T(8,128)(2,1)S(1)} %copy.80, bf16[1,1,544]{1,2,0:T(8,128)(2,1)S(1)} %copy.50, s32[]{:T(128)} %constant.75.clone.1, s32[]{:T(128)} %bitcast.22, s32[]{:T(128)} %constant.75.clone.1) | dynamic-update-slice | bytes 2180 | tf_op jit(solution)/shard_map/vmap(vmap())/scatter | solution.py:84
  97.9 0.1 fusion.79
  98.2 0.2 fusion.7
  98.5 0.3 fusion.75
  98.8 0.3 convolution_bitcast_fusion.1
  99.1 0.6 copy-done.7
  99.8 0.3 fusion.35
  100.1 0.3 convolution_bitcast_fusion
  100.4 0.2 fusion.37
  100.6 0.7 copy.43
  101.3 6.0 %all-to-all-start.1 = ((f32[1,32,4]{2,0,1:T(1,128)}), f32[1,32,4]{2,0,1:T(1,128)S(1)}, u32[]{:S(2)}, u32[]{:S(2)}) async-start(f32[1,32,4]{2,0,1:T(1,128)} %copy.43), calls=%async_computation.1 | async-start | bytes 32768 | tf_op jit(solution)/shard_map/all_to_all | solution.py:159
  107.4 0.6 slice.96
  108.1 0.7 reshape.442
  109.0 4.9 %all-to-all-done.1 = f32[1,32,4]{2,0,1:T(1,128)S(1)} async-done(((f32[1,32,4]{2,0,1:T(1,128)}), f32[1,32,4]{2,0,1:T(1,128)S(1)}, u32[]{:S(2)}, u32[]{:S(2)}) %all-to-all-start.1) | async-done | bytes 544 | tf_op jit(solution)/shard_map/all_to_all | solution.py:159
  113.9 3.3 %all-to-all-start = ((f32[1,32,256]{2,0,1:T(1,128)}), f32[1,32,256]{2,0,1:T(1,128)S(1)}, u32[]{:S(2)}, u32[]{:S(2)}) async-start(f32[1,32,256]{2,0,1:T(1,128)} %reshape.442), calls=%async_computation | async-start | bytes 65536 | tf_op jit(solution)/shard_map/all_to_all | solution.py:155
  118.1 5.7 %all-to-all-done = f32[1,32,256]{2,0,1:T(1,128)S(1)} async-done(((f32[1,32,256]{2,0,1:T(1,128)}), f32[1,32,256]{2,0,1:T(1,128)S(1)}, u32[]{:S(2)}, u32[]{:S(2)}) %all-to-all-start) | async-done | bytes 32800 | tf_op jit(solution)/shard_map/all_to_all | solution.py:155
  123.9 0.2 convolution_convert_fusion
  124.2 10.3 %psum.7 = bf16[5,2048]{1,0:T(8,128)(2,1)S(1)} all-reduce(bf16[5,2048]{1,0:T(8,128)(2,1)S(1)} %convolution_convert_fusion), channel_id=1, replica_groups=mesh['kv'=8,'tp'=4] {'tp'}, use_global_device_ids=true, to_apply=%region_11.12 | all-reduce | flops 10240 | bytes 40960 | tf_op jit(solution)/shard_map/psum | solution.py:183
  134.5 0.6 slice.104
  135.1 0.6 slice.105
  (83 shorter events, 3.6 us)
Async XLA Ops:
  0.6 123.3 %copy-start = (bf16[256,2048]{1,0:T(8,128)(2,1)S(1)}, bf16[256,2048]{1,0:T(8,128)(2,1)}, u32[]{:S(2)}) copy-start(bf16[256,2048]{1,0:T(8,128)(2,1)} %param.35) | copy-start | bytes 3145732
  0.6 3.1 %copy-start.5 = (bf16[2048,128]{1,0:T(8,128)(2,1)S(1)}, bf16[2048,128]{1,0:T(8,128)(2,1)}, u32[]{:S(2)}) copy-start(bf16[2048,128]{1,0:T(8,128)(2,1)} %param.29) | copy-start | bytes 1572868
  0.7 2.9 %copy-start.15 = (bf16[2048,32]{0,1:T(8,128)(2,1)S(1)}, bf16[2048,32]{0,1:T(8,128)(2,1)}, u32[]{:S(2)}) copy-start(bf16[2048,32]{0,1:T(8,128)(2,1)} %param.30) | copy-start | bytes 393220
  0.7 2.7 %copy-start.8 = (bf16[4,2048]{1,0:T(4,128)(2,1)S(1)}, bf16[4,2048]{1,0:T(4,128)(2,1)}, u32[]{:S(2)}) copy-start(bf16[4,2048]{1,0:T(4,128)(2,1)} %param.19) | copy-start | bytes 49156
  0.7 2.7 %copy-start.9 = (bf16[1,2048]{1,0:T(2,128)(2,1)S(1)}, bf16[1,2048]{1,0:T(2,128)(2,1)}, u32[]{:S(2)}) copy-start(bf16[1,2048]{1,0:T(2,128)(2,1)} %param.20) | copy-start | bytes 12292
  0.7 2.9 %copy-start.10 = (f32[2048]{0:T(1024)S(1)}, f32[2048]{0:T(1024)}, u32[]{:S(2)}) copy-start(f32[2048]{0:T(1024)} %param.25) | copy-start | bytes 24580
  2.0 8.3 %copy-start.3 = (bf16[2048,192]{0,1:T(8,128)(2,1)S(1)}, bf16[2048,192]{0,1:T(8,128)(2,1)}, u32[]{:S(2)}) copy-start(bf16[2048,192]{0,1:T(8,128)(2,1)} %param.28) | copy-start | bytes 2359300
  10.3 6.1 %copy-start.6 = (bf16[256,544]{0,1:T(8,128)(2,1)S(1)}, bf16[256,544]{0,1:T(8,128)(2,1)}, u32[]{:S(2)}) copy-start(bf16[256,544]{0,1:T(8,128)(2,1)} %param.23) | copy-start | bytes 835588
  16.6 0.7 copy-start.12
  17.3 31.8 %copy-start.11 = (f32[768]{0:T(1024)S(1)}, f32[768]{0:T(1024)}, u32[]{:S(2)}) copy-start(f32[768]{0:T(1024)} %param.26) | copy-start | bytes 9220
  17.5 62.5 %copy-start.4 = (bf16[768,128]{1,0:T(8,128)(2,1)S(1)}, bf16[768,128]{1,0:T(8,128)(2,1)}, u32[]{:S(2)}) copy-start(bf16[768,128]{1,0:T(8,128)(2,1)} %param.32) | copy-start | bytes 589828
  17.5 62.8 %copy-start.1 = (bf16[768,256]{1,0:T(8,128)(2,1)S(1)}, bf16[768,256]{1,0:T(8,128)(2,1)}, u32[]{:S(2)}) copy-start(bf16[768,256]{1,0:T(8,128)(2,1)} %param.31) | copy-start | bytes 1179652
  81.7 1.0 copy-start.2
  83.9 17.4 %all-to-all-start.2 = ((f32[1,32,4]{2,0,1:T(1,128)}), f32[1,32,4]{2,0,1:T(1,128)S(1)}, u32[]{:S(2)}, u32[]{:S(2)}) async-start(f32[1,32,4]{2,0,1:T(1,128)} %copy.46), calls=%async_computation.2 | async-start | bytes 32768 | tf_op jit(solution)/shard_map/all_to_all | solution.py:158
  89.9 0.7 copy-start.14
  92.1 0.7 copy-start.13
  98.8 1.0 copy-start.7
  101.3 12.6 %all-to-all-start.1 = ((f32[1,32,4]{2,0,1:T(1,128)}), f32[1,32,4]{2,0,1:T(1,128)S(1)}, u32[]{:S(2)}, u32[]{:S(2)}) async-start(f32[1,32,4]{2,0,1:T(1,128)} %copy.43), calls=%async_computation.1 | async-start | bytes 32768 | tf_op jit(solution)/shard_map/all_to_all | solution.py:159
  113.9 10.0 %all-to-all-start = ((f32[1,32,256]{2,0,1:T(1,128)}), f32[1,32,256]{2,0,1:T(1,128)S(1)}, u32[]{:S(2)}, u32[]{:S(2)}) async-start(f32[1,32,256]{2,0,1:T(1,128)} %reshape.442), calls=%async_computation | async-start | bytes 65536 | tf_op jit(solution)/shard_map/all_to_all | solution.py:155
where the time goes:
time: 136 us
  blocking collectives  84.1 us (62%)
  starting transfers between devices  14.8 us (11%)
  local copies, waits for them, and re-layouts  13.7 us (10%)
  waiting for transfers between devices  10.7 us (8%)
  other arithmetic  5.93 us (4%)
  matrix products  4.06 us (3%)
  between operations  2.43 us (2%)
    all_gather x1, blocking collectives, local(): lax.all_gather(piece_rows, 'kv', axis=0, tiled=True)  31.4 us
    all_gather x1, blocking collectives, local(): lax.all_gather(query_lat[:piece_dev], 'kv', axis=0, tiled=True)  30.8 us
    psum x1, blocking collectives, local(): lax.psum(partial_value, 'tp').astype(jnp.float32).astype(jnp.bfloat16)  10.3 us
    all_gather x1, blocking collectives, local(): lax.all_gather(latent_comp, 'tp', axis=1, tiled=True)  6.16 us
    all_to_all x1, starting transfers between devices, local(): lax.all_to_all(local_peak[None], 'kv', split_axis=1, concat_axis=0, tiled...  6 us
    all_to_all x1, waiting for transfers between devices, local(): lax.all_to_all(partial_sum.reshape(1, piece_total, -1), 'kv', split_axis=...  5.73 us
    all_gather x1, blocking collectives, local(): lax.all_gather(query_comp, 'tp', axis=1, tiled=True)  5.5 us
    all_to_all x1, starting transfers between devices, local(): lax.all_to_all(weight_sum[None], 'kv', split_axis=1, concat_axis=0, tiled...  5.43 us
  transfers between devices with their start and end apart: 3, of which 2 were waited for; matrix products, arithmetic and copies ran while one was open for 9% of the time, Pallas kernels for 0%

commit v1 on v0

--- a/solution.py
+++ b/solution.py
@@ -1,3 +1,4 @@
+import functools
 import jax
 import jax.numpy as jnp
 from jax import lax
@@ -8,6 +9,18 @@
 NEG_FILL = -1e30
 RMS_EPS = 1e-06
 THETA = 10000.0
+
+
+def divide_steps_all(unit, dimension_no, in_dim):
+    return jnp.concatenate(
+        jax.lax.all_to_all(
+            jnp.stack(jnp.split(unit, jax.lax.psum(1, "kv"), dimension_no), axis=0), "kv", 0, 0
+        ),
+        in_dim,
+    )
+
+
+_write_wall = functools.partial(divide_steps_all, dimension_no=1, in_dim=0)
 
 
 def rms_scale(values, gain_row):
@@ -156,7 +169,7 @@
             partial_sum.reshape(1, piece_total, -1), "kv", split_axis=1, concat_axis=0, tiled=True
         ),
         lax.all_to_all(weight_sum[None], "kv", split_axis=1, concat_axis=0, tiled=True),
-        lax.all_to_all(local_peak[None], "kv", split_axis=1, concat_axis=0, tiled=True),
+        _write_wall(local_peak[None]),
     )
     global_peak = jnp.max(all_peaks, axis=0)
     factor = jnp.exp(all_peaks - global_peak[None])

time: 136 us -> 141 us (1.037)
  local copies, waits for them, and re-layouts: 13.7 us -> 18.2 us
    unnamed x40 -> x46, local copies, waits for them, and re-layouts: 5.09 us -> 9.07 us
  transfers between devices with their start and end apart: 3 -> 3, of which waited for: 2 -> 2; matrix products, arithmetic and copies ran while one was open for 9% -> 12% of each run, Pallas kernels for 0% -> 0%
where the time goes in v1:
time: 141 us; the launch traced here: 140 us
  blocking collectives  84.1 us (60%)
  local copies, waits for them, and re-layouts  18.2 us (13%)
  starting transfers between devices  14.8 us (10%)
  waiting for transfers between devices  10.8 us (8%)
  other arithmetic  6.06 us (4%)
  matrix products  4.06 us (3%)
  between operations  2.44 us (2%)
    all_gather x1, blocking collectives, local(): lax.all_gather(piece_rows, 'kv', axis=0, tiled=True)  31.4 us
    all_gather x1, blocking collectives, local(): lax.all_gather(query_lat[:piece_dev], 'kv', axis=0, tiled=True)  30.8 us
    psum x1, blocking collectives, local(): lax.psum(partial_value, 'tp').astype(jnp.float32).astype(jnp.bfloat16)  10.3 us
    unnamed x46, local copies, waits for them, and re-layouts  9.07 us
    all_gather x1, blocking collectives, local(): lax.all_gather(latent_comp, 'tp', axis=1, tiled=True)  6.16 us
    all_to_all x1, starting transfers between devices, divide_steps_all(): jax.lax.all_to_all(jnp.stack(jnp.split(unit, jax.lax.psum(1, 'kv'), dimen...  6.01 us
    all_to_all x1, waiting for transfers between devices, local(): lax.all_to_all(partial_sum.reshape(1, piece_total, -1), 'kv', split_axis=...  5.85 us
    all_gather x1, blocking collectives, local(): lax.all_gather(query_comp, 'tp', axis=1, tiled=True)  5.5 us
  transfers between devices with their start and end apart: 3, of which 2 were waited for; matrix products, arithmetic and copies ran while one was open for 12% of the time, Pallas kernels for 0%

profile of v1, /device:TPU:0, one launch (start us, length us, event | category | flops | bytes accessed | tf_op | source)
XLA Modules:
  0.0 140.5 jit_solution(11163216246703736530)
XLA Ops:
  0.7 1.3 copy.113
  3.6 0.2 convolution_convert_fusion.6
  3.8 0.2 convolution_convert_fusion.5
  4.0 6.2 %all_gather.14 = bf16[5,512]{1,0:T(8,128)(2,1)S(1)} all-gather(bf16[5,128]{1,0:T(8,128)(2,1)S(1)} %convolution_convert_fusion.5), channel_id=1, replica_groups=mesh['kv'=8,'tp'=4] {'tp'}, dimensions={1}, use_global_device_ids=true | all-gather | bytes 6400 | tf_op jit(solution)/shard_map/all_gather | solution.py:135
  10.3 0.3 fusion.5
  10.6 5.5 %all-gather = bf16[4,192,5]{1,2,0:T(8,128)(2,1)S(1)} all-gather(bf16[1,192,5]{1,2,0:T(8,128)(2,1)S(1)} %fusion.5), channel_id=1, replica_groups=mesh['kv'=8,'tp'=4] {'tp'}, dimensions={0}, use_global_device_ids=true | all-gather | bytes 9600 | tf_op jit(solution)/shard_map/all_gather | solution.py:134
  16.4 0.2 copy.57
  16.7 0.6 copy-done.12
  17.6 31.4 %all-gather.2 = bf16[8,4,544]{2,1,0:T(4,128)(2,1)S(1)} all-gather(bf16[1,4,544]{2,1,0:T(4,128)(2,1)S(1)} %slice_bitcast_fusion.14), channel_id=1, replica_groups=mesh['kv'=8,'tp'=4] {'kv'}, dimensions={0}, use_global_device_ids=true | all-gather | bytes 39168 | tf_op jit(solution)/shard_map/all_gather | solution.py:149
  49.2 30.8 %all-gather.1 = bf16[8,4,768]{2,1,0:T(4,128)(2,1)S(1)} all-gather(bf16[1,4,768]{2,1,0:T(4,128)(2,1)S(1)} %slice_bitcast_fusion.10), channel_id=1, replica_groups=mesh['kv'=8,'tp'=4] {'kv'}, dimensions={0}, use_global_device_ids=true | all-gather | bytes 55296 | tf_op jit(solution)/shard_map/all_gather | solution.py:148
  80.9 0.9 fusion.10
  81.7 0.2 fusion.22
  81.9 0.7 copy-done.2
  82.7 0.4 fusion.79
  83.2 0.7 copy.73
  83.9 5.4 %all-to-all-start.2 = ((f32[1,32,4]{2,0,1:T(1,128)}), f32[1,32,4]{2,0,1:T(1,128)S(1)}, u32[]{:S(2)}, u32[]{:S(2)}) async-start(f32[1,32,4]{2,0,1:T(1,128)} %copy.73), calls=%async_computation.2 | async-start | bytes 32768 | tf_op jit(solution)/shard_map/all_to_all | solution.py:171
  89.7 0.2 fusion.11
  89.9 0.6 copy-done.14
  90.7 0.6 fusion.77
  91.3 0.8 constant_dynamic-slice_fusion
  92.1 0.7 copy-done.13
  92.8 2.0 %and_reduce_fusion = pred[]{:T(512)} fusion(s32[3]{0:T(128)S(1)} %copy-done.13, s32[1]{0:T(128)} %bitcast.28, s32[1]{0:T(128)} %bitcast.27, s32[1]{0:T(128)} %constant.79.clone.1), kind=kLoop, calls=%fused_computation.117 | loop fusion | flops 17 | bytes 25 | tf_op jit(solution)/shard_map/reduce.1
  94.8 1.2 broadcast_select_fusion
  96.2 1.6 %scatter.4 = bf16[1,768,544]{1,2,0:T(8,128)(2,1)S(1)} dynamic-update-slice(bf16[1,768,544]{1,2,0:T(8,128)(2,1)S(1)} %copy.113, bf16[1,1,544]{1,2,0:T(8,128)(2,1)S(1)} %copy.77, s32[]{:T(128)} %constant.75.clone.1, s32[]{:T(128)} %bitcast.30, s32[]{:T(128)} %constant.75.clone.1) | dynamic-update-slice | bytes 2180 | tf_op jit(solution)/shard_map/vmap(vmap())/scatter | solution.py:97
  98.2 0.2 fusion.7
  98.5 0.3 fusion.78
  98.8 0.3 convolution_bitcast_fusion.1
  99.1 0.6 copy-done.7
  99.8 0.3 fusion.36
  100.1 0.3 convolution_bitcast_fusion
  100.6 0.6 constant_dynamic-update-slice_fusion.7
  101.8 0.6 constant_dynamic-update-slice_fusion.6
  102.4 0.6 constant_dynamic-update-slice_fusion.5
  103.0 0.6 constant_dynamic-update-slice_fusion.4
  103.6 0.6 constant_dynamic-update-slice_fusion.3
  104.2 0.6 constant_dynamic-update-slice_fusion.2
  104.8 0.6 constant_dynamic-update-slice_fusion.1
  105.3 0.6 constant_dynamic-update-slice_fusion
  106.1 6.0 %all-to-all-start.1 = ((f32[8,1,4,4]{3,2,1,0:T(4,128)}), f32[8,1,4,4]{3,2,1,0:T(4,128)S(1)}, u32[]{:S(2)}, u32[]{:S(2)}) async-start(f32[8,1,4,4]{3,2,1,0:T(4,128)} %constant_dynamic-update-slice_fusion), calls=%async_computation.1 | async-start | bytes 32768 | tf_op jit(solution)/shard_map/all_to_all | solution.py:16
  112.2 0.6 slice.96
  112.9 0.7 reshape.446
  113.7 5.0 %all-to-all-done.1 = f32[8,1,4,4]{3,2,1,0:T(4,128)S(1)} async-done(((f32[8,1,4,4]{3,2,1,0:T(4,128)}), f32[8,1,4,4]{3,2,1,0:T(4,128)S(1)}, u32[]{:S(2)}, u32[]{:S(2)}) %all-to-all-start.1) | async-done | bytes 544 | tf_op jit(solution)/shard_map/all_to_all | solution.py:16
  118.7 3.3 %all-to-all-start = ((f32[1,32,256]{2,0,1:T(1,128)}), f32[1,32,256]{2,0,1:T(1,128)S(1)}, u32[]{:S(2)}, u32[]{:S(2)}) async-start(f32[1,32,256]{2,0,1:T(1,128)} %reshape.446), calls=%async_computation | async-start | bytes 65536 | tf_op jit(solution)/shard_map/all_to_all | solution.py:168
  122.8 5.8 %all-to-all-done = f32[1,32,256]{2,0,1:T(1,128)S(1)} async-done(((f32[1,32,256]{2,0,1:T(1,128)}), f32[1,32,256]{2,0,1:T(1,128)S(1)}, u32[]{:S(2)}, u32[]{:S(2)}) %all-to-all-start) | async-done | bytes 32800 | tf_op jit(solution)/shard_map/all_to_all | solution.py:168
  128.7 0.2 convolution_convert_fusion
  129.0 10.3 %psum.7 = bf16[5,2048]{1,0:T(8,128)(2,1)S(1)} all-reduce(bf16[5,2048]{1,0:T(8,128)(2,1)S(1)} %convolution_convert_fusion), channel_id=1, replica_groups=mesh['kv'=8,'tp'=4] {'tp'}, use_global_device_ids=true, to_apply=%region_11.12 | all-reduce | flops 10240 | bytes 40960 | tf_op jit(solution)/shard_map/psum | solution.py:196
  139.3 0.6 slice.104
  139.9 0.6 slice.105
  (97 shorter events, 5.4 us)
Async XLA Ops:
  0.6 128.1 %copy-start = (bf16[256,2048]{1,0:T(8,128)(2,1)S(1)}, bf16[256,2048]{1,0:T(8,128)(2,1)}, u32[]{:S(2)}) copy-start(bf16[256,2048]{1,0:T(8,128)(2,1)} %param.35) | copy-start | bytes 3145732
  0.6 3.1 %copy-start.5 = (bf16[2048,128]{1,0:T(8,128)(2,1)S(1)}, bf16[2048,128]{1,0:T(8,128)(2,1)}, u32[]{:S(2)}) copy-start(bf16[2048,128]{1,0:T(8,128)(2,1)} %param.29) | copy-start | bytes 1572868
  0.7 2.9 %copy-start.15 = (bf16[2048,32]{0,1:T(8,128)(2,1)S(1)}, bf16[2048,32]{0,1:T(8,128)(2,1)}, u32[]{:S(2)}) copy-start(bf16[2048,32]{0,1:T(8,128)(2,1)} %param.30) | copy-start | bytes 393220
  0.7 2.7 %copy-start.8 = (bf16[4,2048]{1,0:T(4,128)(2,1)S(1)}, bf16[4,2048]{1,0:T(4,128)(2,1)}, u32[]{:S(2)}) copy-start(bf16[4,2048]{1,0:T(4,128)(2,1)} %param.19) | copy-start | bytes 49156
  0.7 2.7 %copy-start.9 = (bf16[1,2048]{1,0:T(2,128)(2,1)S(1)}, bf16[1,2048]{1,0:T(2,128)(2,1)}, u32[]{:S(2)}) copy-start(bf16[1,2048]{1,0:T(2,128)(2,1)} %param.20) | copy-start | bytes 12292
  0.7 2.9 %copy-start.10 = (f32[2048]{0:T(1024)S(1)}, f32[2048]{0:T(1024)}, u32[]{:S(2)}) copy-start(f32[2048]{0:T(1024)} %param.25) | copy-start | bytes 24580
  2.0 8.3 %copy-start.3 = (bf16[2048,192]{0,1:T(8,128)(2,1)S(1)}, bf16[2048,192]{0,1:T(8,128)(2,1)}, u32[]{:S(2)}) copy-start(bf16[2048,192]{0,1:T(8,128)(2,1)} %param.28) | copy-start | bytes 2359300
  10.3 6.1 %copy-start.6 = (bf16[256,544]{0,1:T(8,128)(2,1)S(1)}, bf16[256,544]{0,1:T(8,128)(2,1)}, u32[]{:S(2)}) copy-start(bf16[256,544]{0,1:T(8,128)(2,1)} %param.23) | copy-start | bytes 835588
  16.6 0.7 copy-start.12
  17.3 31.8 %copy-start.11 = (f32[768]{0:T(1024)S(1)}, f32[768]{0:T(1024)}, u32[]{:S(2)}) copy-start(f32[768]{0:T(1024)} %param.26) | copy-start | bytes 9220
  17.5 62.5 %copy-start.4 = (bf16[768,128]{1,0:T(8,128)(2,1)S(1)}, bf16[768,128]{1,0:T(8,128)(2,1)}, u32[]{:S(2)}) copy-start(bf16[768,128]{1,0:T(8,128)(2,1)} %param.32) | copy-start | bytes 589828
  17.5 62.8 %copy-start.1 = (bf16[768,256]{1,0:T(8,128)(2,1)S(1)}, bf16[768,256]{1,0:T(8,128)(2,1)}, u32[]{:S(2)}) copy-start(bf16[768,256]{1,0:T(8,128)(2,1)} %param.31) | copy-start | bytes 1179652
  81.7 1.0 copy-start.2
  83.9 22.2 %all-to-all-start.2 = ((f32[1,32,4]{2,0,1:T(1,128)}), f32[1,32,4]{2,0,1:T(1,128)S(1)}, u32[]{:S(2)}, u32[]{:S(2)}) async-start(f32[1,32,4]{2,0,1:T(1,128)} %copy.73), calls=%async_computation.2 | async-start | bytes 32768 | tf_op jit(solution)/shard_map/all_to_all | solution.py:171
  89.9 0.7 copy-start.14
  92.1 0.7 copy-start.13
  98.8 1.0 copy-start.7
  106.1 12.6 %all-to-all-start.1 = ((f32[8,1,4,4]{3,2,1,0:T(4,128)}), f32[8,1,4,4]{3,2,1,0:T(4,128)S(1)}, u32[]{:S(2)}, u32[]{:S(2)}) async-start(f32[8,1,4,4]{3,2,1,0:T(4,128)} %constant_dynamic-update-slice_fusion), calls=%async_computation.1 | async-start | bytes 32768 | tf_op jit(solution)/shard_map/all_to_all | solution.py:16
  118.7 10.0 %all-to-all-start = ((f32[1,32,256]{2,0,1:T(1,128)}), f32[1,32,256]{2,0,1:T(1,128)S(1)}, u32[]{:S(2)}, u32[]{:S(2)}) async-start(f32[1,32,256]{2,0,1:T(1,128)} %reshape.446), calls=%async_computation | async-start | bytes 65536 | tf_op jit(solution)/shard_map/all_to_all | solution.py:168
